TPU v7x, 256 devices: a 4x2x16 block of a 4x16x16 slice. The times are simulated.
256 devices in a mesh: grp: 2 (over y), sp: 16 (over z), tp: 8 (over x, core).
Axes of the slice: x: 4, y: 2, z: 16, core: 2. Of those that a mesh axis runs over, the one named last changes fastest.
The devices are a block of a 4x16x16 slice.
Arguments:
- tokens: bfloat16 [32, 4096, 4096], P(('grp', 'tp'), 'sp'), parts along dimension 0, may hold values from -8 to 8, as said below
- offsets: int32 [32], P(('grp', 'tp')), parts along dimension 0, may hold values from 0 to 4095
- in_gain: float32 [4096], replicated, may hold values from 0.1 to 1.9
- w_latent: bfloat16 [4096, 1024], P('sp'), may hold values from -0.09375 to 0.09375
- w_rope_key: bfloat16 [4096, 32], replicated, may hold values from -0.09375 to 0.09375
- kv_gain: float32 [1024], replicated, may hold values from 0.1 to 1.9
- w_up_key: bfloat16 [1024, 2048], P(None, 'tp'), may hold values from -0.1875 to 0.1875
- w_up_value: bfloat16 [1024, 2048], P(None, 'tp'), may hold values from -0.1875 to 0.1875
- q_nope: bfloat16 [32, 2048], P(('grp', 'sp'), 'tp'), parts along dimension 0, may hold values from -300 to 300, as said below
- q_rope: bfloat16 [32, 1024], P(('grp', 'sp'), 'tp'), parts along dimension 0, may hold values from -16 to 16
Outputs:
- keys: bfloat16 [32, 4096, 2048], P(('grp', 'sp'), None, 'tp'), parts along dimension 0
- values: bfloat16 [32, 4096, 2048], P(('grp', 'sp'), None, 'tp'), parts along dimension 0
- rope_keys: bfloat16 [32, 32, 4096], P(('grp', 'sp')), parts along dimension 0
- read: bfloat16 [32, 2048], P(('grp', 'sp'), 'tp'), parts along dimension 0
There are 2 independent parts, one for each index of `grp`. A program takes and returns all parts, laid end to end along the dimension named above; an argument that names none is the same for every part. Nothing has to cross between parts.
Inputs may be any that keep to these rules, and one draw needn't show every extreme that they name: `tokens`: entries of the layer's input. `q_nope`: entries of the first decoding token's queries.
All inputs are finite; a program needn't handle non-finite values.
Results may differ from a plain program's by a relative error of at most 0.02.
Values may be sent and summed in bfloat16 or wider, within the bound.
A program may use at most 128 MiB of HBM per device.

v0:
```python
import jax
import jax.numpy as jnp
from jax import lax
from jax.sharding import PartitionSpec as P

HEAD = 64
ROPE = 32
EPS = 1e-06


def joined_along(tiles, dim):
    shape = list(tiles.shape[1:])
    shape[dim] *= tiles.shape[0]
    return jnp.moveaxis(tiles, 0, dim).reshape(shape)


def copy_for_each(value, axis):
    peers = lax.axis_size(axis)
    return lax.all_to_all(
        jnp.broadcast_to(value[None], (peers, *value.shape)), axis, 0, 0, tiled=True
    )


def gather_directly(value, axis, dim):
    return joined_along(copy_for_each(value, axis), dim)


def rms_scale(values, gain):
    wide = values.astype(jnp.float32)
    return wide * lax.rsqrt(jnp.mean(wide * wide, axis=-1, keepdims=True) + EPS) * gain


def rotate(raw, position):
    inverse = 10000.0 ** (-jnp.arange(0, ROPE, 2).astype(jnp.float32) / ROPE)
    angle = position.astype(jnp.float32)[..., None] * inverse
    cosine, sine = (jnp.cos(angle), jnp.sin(angle))
    half = ROPE // 2
    first, second = (raw[..., :half], raw[..., half:])
    return jnp.concatenate(
        [first * cosine - second * sine, second * cosine + first * sine], axis=-1
    )


def local(
    tokens, offsets, in_gain, w_latent, w_rope_key, kv_gain, w_up_key, w_up_value, q_nope, q_rope
):
    prompts, rows, width = tokens.shape
    n_sp = lax.axis_size("sp")
    length = n_sp * rows
    block = lax.axis_index("sp")
    normed = rms_scale(tokens.reshape(prompts * rows, width), in_gain).astype(jnp.bfloat16)
    latent_raw = jnp.dot(
        normed,
        lax.all_gather(w_latent, "sp", axis=0, tiled=True),
        preferred_element_type=jnp.float32,
    )
    latent = rms_scale(latent_raw, kv_gain).astype(jnp.bfloat16)
    position = offsets[:, None] + block * rows + jnp.arange(rows, dtype=jnp.int32)[None, :]
    rope_raw = jnp.dot(normed, w_rope_key, preferred_element_type=jnp.float32).reshape(
        prompts, rows, ROPE
    )
    rotated = rotate(rope_raw, position).astype(jnp.bfloat16)
    head_cols = w_up_key.shape[1]
    paired = jnp.stack([w_up_key, w_up_value])
    both = jnp.einsum(
        "tk,skc->stc",
        latent,
        lax.all_gather(paired, "tp", axis=2, tiled=True),
        preferred_element_type=jnp.float32,
    ).astype(jnp.bfloat16)
    both = both.reshape(2, prompts, rows, both.shape[2])
    by_head = lax.all_to_all(both, "tp", split_axis=3, concat_axis=1, tiled=True)
    rope_every = gather_directly(rotated, "tp", 0)
    moved, rope_moved = (
        lax.all_to_all(by_head[:, :, None], "sp", split_axis=1, concat_axis=2, tiled=True),
        lax.all_to_all(rope_every[None, :, None], "sp", split_axis=1, concat_axis=2, tiled=True),
    )
    keys = moved[0].reshape(length, head_cols)
    values = moved[1].reshape(length, head_cols)
    rope_all = rope_moved.reshape(length, ROPE)
    rope_keys = rope_all.T
    heads_here = head_cols // HEAD
    query = q_nope.reshape(heads_here, HEAD)
    rotary_q = q_rope.reshape(heads_here, ROPE)
    keys_split = keys.reshape(length, heads_here, HEAD)
    scores = jnp.einsum("hd,jhd->hj", query, keys_split, preferred_element_type=jnp.float32)
    scores = scores + jnp.dot(rotary_q, rope_keys, preferred_element_type=jnp.float32)
    scores = scores / jnp.sqrt(jnp.float32(HEAD + ROPE))
    peak = jnp.max(scores, axis=-1, keepdims=True)
    expo = jnp.exp(scores - peak)
    weights = (expo / jnp.sum(expo, axis=-1, keepdims=True)).astype(jnp.bfloat16)
    read = jnp.einsum(
        "hj,jhd->hd",
        weights,
        values.reshape(length, heads_here, HEAD),
        preferred_element_type=jnp.float32,
    )
    read = read.astype(jnp.bfloat16).reshape(1, heads_here * HEAD)
    return (keys[None], values[None], rope_keys[None], read)


def solution(mesh):
    in_specs = (
        P(("grp", "tp"), "sp", None),
        P(("grp", "tp")),
        P(),
        P("sp", None),
        P(),
        P(),
        P(None, "tp"),
        P(None, "tp"),
        P(("grp", "sp"), "tp"),
        P(("grp", "sp"), "tp"),
    )
    out_specs = (
        P(("grp", "sp"), None, "tp"),
        P(("grp", "sp"), None, "tp"),
        P(("grp", "sp"), None, None),
        P(("grp", "sp"), "tp"),
    )
    return jax.shard_map(local, mesh=mesh, in_specs=in_specs, out_specs=out_specs, check_vma=False)
```

profile of v0, /device:TPU:33, one launch (start us, length us, event | category | flops | bytes accessed | tf_op | source)
XLA Modules:
  0.0 515.6 jit_solution(11231751343885072324)
XLA Ops:
  7.2 0.0 copy-start
  7.2 0.1 all-gather.5.cloned.1.call-start
  7.3 0.7 all-gather.5.cloned.1.call-update
  8.0 0.1 all-gather.3.cloned.1.call-start
  8.1 2.3 pad_maximum_fusion
  10.3 0.1 all-gather.3.cloned.1.call-update
  10.4 0.0 copy-start.3
  10.4 0.8 broadcast_add_fusion
  11.2 0.1 add_convert_fusion
  11.3 3.3 multiply_reduce_fusion
  14.7 1.4 fusion.4
  16.1 0.2 fusion.21
  16.4 0.8 broadcast_in_dim.7
  17.2 23.7 %all-to-all-start.2 = ((bf16[8,2,256,32]{2,1,3,0:T(2,128)(2,1)}), bf16[8,2,256,32]{2,1,3,0:T(2,128)(2,1)S(1)}, u32[]{:S(2)}, u32[]{:S(2)}) async-start(bf16[8,2,256,32]{2,1,3,0:T(2,128)(2,1)} %broadcast_in_dim.7), calls=%async_computation.2 | async-start | bytes 524288 | tf_op jit(solution)/shard_map/all_to_all | solution.py:19
  40.9 5.8 %fusion.1 = bf16[512,4096]{1,0:T(8,128)(2,1)} fusion(bf16[2,256,4096]{2,1,0:T(8,128)(2,1)} %param.10, f32[4096]{0:T(1024)S(1)} %copy-done.6, f32[512]{0:T(512)S(1)} %bitcast.76), kind=kLoop, calls=%fused_computation.2 | loop fusion | flops 8388608 | bytes 8407040 | tf_op jit(solution)/shard_map/convert_element_type | solution.py:51
  46.7 81.6 %all-gather.5.cloned.1.call-done = bf16[4096,1024]{1,0:T(8,128)(2,1)} async-done(((bf16[256,1024]{1,0:T(8,128)(2,1)}), bf16[4096,1024]{1,0:T(8,128)(2,1)}) %all-gather.5.cloned.1.call-update) | async-done | bytes 8388624 | tf_op jit(solution)/shard_map/all_gather | solution.py:54
  128.3 8.3 %multiply_reduce_fusion.1 = (f32[512]{0:T(512)S(1)}, f32[512,1024]{1,0:T(8,128)S(1)}) fusion(bf16[512,4096]{1,0:T(8,128)(2,1)} %fusion.1, bf16[4096,1024]{1,0:T(8,128)(2,1)} %all-gather.5.cloned.1.call-done), kind=kOutput, calls=%fused_computation.14 | convolution fusion | flops 4296015360 | bytes 14682112 | tf_op jit(solution)/shard_map/dot_general | solution.py:52
  136.6 52.3 %all-gather.3.cloned.1.call-done = bf16[2,1024,2048]{2,1,0:T(8,128)(2,1)} async-done(((bf16[2,1024,256]{2,1,0:T(8,128)(2,1)}), bf16[2,1024,2048]{2,1,0:T(8,128)(2,1)}) %all-gather.3.cloned.1.call-update) | async-done | bytes 8388624 | tf_op jit(solution)/shard_map/all_gather | solution.py:68
  188.9 9.6 %convolution_convert_fusion = bf16[2,2048,512]{1,2,0:T(8,128)(2,1)} fusion(bf16[2,1024,2048]{2,1,0:T(8,128)(2,1)} %all-gather.3.cloned.1.call-done, f32[512,1024]{1,0:T(8,128)S(1)} %get-tuple-element.11, f32[1024]{0:T(1024)S(1)} %copy-done.8, f32[512]{0:T(512)S(1)} %add_rsqrt_fusion), kind=kOutput, calls=%fused_computation.12 | convolution fusion | flops 4298637312 | bytes 14686208 | tf_op jit(solution)/shard_map/tk,skc->stc/dot_general | solution.py:65
  198.6 11.2 %copy.25 = bf16[2,2,256,2048]{2,1,0,3:T(2,128)(2,1)} copy(bf16[2,2,256,2048]{3,2,1,0:T(8,128)(2,1)} %bitcast.68) | data formatting | bytes 8388608 | tf_op jit(solution)/shard_map/reshape | solution.py:71
  209.8 4.7 all-to-all-start
  214.4 0.7 copy.30
  215.2 48.1 %all-to-all-done = bf16[2,2,256,2048]{2,1,0,3:T(2,128)(2,1)} async-done(((bf16[2,2,256,2048]{2,1,0,3:T(2,128)(2,1)}), bf16[2,2,256,2048]{2,1,0,3:T(2,128)(2,1)}, u32[]{:S(2)}, u32[]{:S(2)}) %all-to-all-start) | async-done | bytes 4194336 | tf_op jit(solution)/shard_map/all_to_all | solution.py:72
  263.3 12.1 %all-to-all-start.3 = ((bf16[1,16,1,256,32]{3,4,2,0,1:T(8,128)(2,1)}), bf16[1,16,1,256,32]{3,4,2,0,1:T(8,128)(2,1)S(1)}, u32[]{:S(2)}, u32[]{:S(2)}) async-start(bf16[1,16,1,256,32]{3,4,2,0,1:T(8,128)(2,1)} %bitcast.13), calls=%async_computation.3 | async-start | bytes 524288 | tf_op jit(solution)/shard_map/all_to_all | solution.py:76
  275.4 4.9 copy.26
  280.4 7.7 %all-to-all-done.3 = bf16[1,16,1,256,32]{3,4,2,0,1:T(8,128)(2,1)S(1)} async-done(((bf16[1,16,1,256,32]{3,4,2,0,1:T(8,128)(2,1)}), bf16[1,16,1,256,32]{3,4,2,0,1:T(8,128)(2,1)S(1)}, u32[]{:S(2)}, u32[]{:S(2)}) %all-to-all-start.3) | async-done | bytes 262176 | tf_op jit(solution)/shard_map/all_to_all | solution.py:76
  288.1 11.6 %all-to-all-start.1 = ((bf16[2,16,1,256,256]{3,4,2,0,1:T(8,128)(2,1)}), bf16[2,16,1,256,256]{3,4,2,0,1:T(8,128)(2,1)}, u32[]{:S(2)}, u32[]{:S(2)}) async-start(bf16[2,16,1,256,256]{3,4,2,0,1:T(8,128)(2,1)} %bitcast.67), calls=%async_computation.1 | async-start | bytes 8388608 | tf_op jit(solution)/shard_map/all_to_all | solution.py:75
  299.7 0.1 reshape.142
  299.8 0.5 broadcast.98
  300.3 0.7 reduce.5
  301.0 0.1 reshape.132
  301.1 0.0 copy-start.5
  301.1 180.2 %all-to-all-done.1 = bf16[2,16,1,256,256]{3,4,2,0,1:T(8,128)(2,1)} async-done(((bf16[2,16,1,256,256]{3,4,2,0,1:T(8,128)(2,1)}), bf16[2,16,1,256,256]{3,4,2,0,1:T(8,128)(2,1)}, u32[]{:S(2)}, u32[]{:S(2)}) %all-to-all-start.1) | async-done | bytes 4194336 | tf_op jit(solution)/shard_map/all_to_all | solution.py:75
  481.3 2.6 fusion.26
  483.9 0.0 copy-start.2
  483.9 1.3 copy-done.2
  485.2 2.5 copy.34
  487.8 3.9 copy.40
  491.7 2.5 copy.33
  494.2 2.4 copy.39
  496.5 4.3 reshape_reshape_squeeze.6
  500.9 2.0 fusion.28
  502.8 0.3 fusion.27
  503.1 0.2 fusion.15
  503.3 0.1 fusion.24
  503.5 2.3 reshape_reshape_squeeze.7
  505.8 2.2 fusion.13
  508.0 0.7 reshape.133
  (25 shorter events, 0.1 us)
Async XLA Ops:
  7.2 7.4 %copy-start = (bf16[4096,32]{0,1:T(8,128)(2,1)S(1)}, bf16[4096,32]{0,1:T(8,128)(2,1)}, u32[]{:S(2)}) copy-start(bf16[4096,32]{0,1:T(8,128)(2,1)} %param.14) | copy-start | bytes 786436
  7.2 7.4 %copy-start.6 = (f32[4096]{0:T(1024)S(1)}, f32[4096]{0:T(1024)}, u32[]{:S(2)}) copy-start(f32[4096]{0:T(1024)} %param.12) | copy-start | bytes 49156
  7.2 121.1 %all-gather.5.cloned.1.call-start = ((), (), s32[]{:S(2)}) async-start(), calls=%async_computation.5 | async-start | bytes 8912896 | tf_op jit(solution)/shard_map/all_gather | solution.py:54
  8.0 180.9 %all-gather.3.cloned.1.call-start = ((), (), s32[]{:S(2)}) async-start(), calls=%async_computation.4 | async-start | bytes 9437184 | tf_op jit(solution)/shard_map/all_gather | solution.py:68
  10.4 4.2 copy-start.3
  17.2 192.6 %all-to-all-start.2 = ((bf16[8,2,256,32]{2,1,3,0:T(2,128)(2,1)}), bf16[8,2,256,32]{2,1,3,0:T(2,128)(2,1)S(1)}, u32[]{:S(2)}, u32[]{:S(2)}) async-start(bf16[8,2,256,32]{2,1,3,0:T(2,128)(2,1)} %broadcast_in_dim.7), calls=%async_computation.2 | async-start | bytes 524288 | tf_op jit(solution)/shard_map/all_to_all | solution.py:19
  46.7 142.2 %copy-start.8 = (f32[1024]{0:T(1024)S(1)}, f32[1024]{0:T(1024)}, u32[]{:S(2)}) copy-start(f32[1024]{0:T(1024)} %param.15) | copy-start | bytes 12292
  209.8 53.6 %all-to-all-start = ((bf16[2,2,256,2048]{2,1,0,3:T(2,128)(2,1)}), bf16[2,2,256,2048]{2,1,0,3:T(2,128)(2,1)}, u32[]{:S(2)}, u32[]{:S(2)}) async-start(bf16[2,2,256,2048]{2,1,0,3:T(2,128)(2,1)} %copy.25), calls=%async_computation | async-start | bytes 8388608 | tf_op jit(solution)/shard_map/all_to_all | solution.py:72
  263.3 24.8 %all-to-all-start.3 = ((bf16[1,16,1,256,32]{3,4,2,0,1:T(8,128)(2,1)}), bf16[1,16,1,256,32]{3,4,2,0,1:T(8,128)(2,1)S(1)}, u32[]{:S(2)}, u32[]{:S(2)}) async-start(bf16[1,16,1,256,32]{3,4,2,0,1:T(8,128)(2,1)} %bitcast.13), calls=%async_computation.3 | async-start | bytes 524288 | tf_op jit(solution)/shard_map/all_to_all | solution.py:76
  288.1 11.6 %copy-start.7 = (bf16[1,256]{1,0:T(2,128)(2,1)S(1)}, bf16[1,256]{1,0:T(2,128)(2,1)}, u32[]{:S(2)}) copy-start(bf16[1,256]{1,0:T(2,128)(2,1)} %param.18) | copy-start | bytes 1540
  288.1 12.2 %copy-start.9 = (bf16[1,128]{1,0:T(2,128)(2,1)S(1)}, bf16[1,128]{1,0:T(2,128)(2,1)}, u32[]{:S(2)}) copy-start(bf16[1,128]{1,0:T(2,128)(2,1)} %param.19) | copy-start | bytes 772
  288.1 193.2 %all-to-all-start.1 = ((bf16[2,16,1,256,256]{3,4,2,0,1:T(8,128)(2,1)}), bf16[2,16,1,256,256]{3,4,2,0,1:T(8,128)(2,1)}, u32[]{:S(2)}, u32[]{:S(2)}) async-start(bf16[2,16,1,256,256]{3,4,2,0,1:T(8,128)(2,1)} %bitcast.67), calls=%async_computation.1 | async-start | bytes 8388608 | tf_op jit(solution)/shard_map/all_to_all | solution.py:75
  301.1 201.8 %copy-start.5 = (bf16[4,8,16,256]{3,1,2,0:T(8,128)(2,1)}, bf16[4,8,16,256]{3,1,2,0:T(8,128)(2,1)S(1)}, u32[]{:S(2)}) copy-start(bf16[4,8,16,256]{3,1,2,0:T(8,128)(2,1)S(1)} %copy.44) | copy-start | bytes 786436
  483.9 1.3 copy-start.2
  496.5 6.9 %copy-start.4 = (bf16[1,16,1,256,256]{3,1,4,2,0:T(8,128)(2,1)S(1)}, bf16[1,16,1,256,256]{3,1,4,2,0:T(8,128)(2,1)}, u32[]{:S(2)}) copy-start(bf16[1,16,1,256,256]{3,1,4,2,0:T(8,128)(2,1)} %copy.34) | copy-start | bytes 6291460
  496.5 12.2 %copy-start.1 = (bf16[4096,32]{0,1:T(8,128)(2,1)S(1)}, bf16[4096,32]{0,1:T(8,128)(2,1)}, u32[]{:S(2)}) copy-start(bf16[4096,32]{0,1:T(8,128)(2,1)} %param.14) | copy-start | bytes 786436
Sparse Core Ops, SparseCore 0:
  9.8 118.4 all-gather.4
  130.7 58.1 all-gather.2
where the time goes:
time: 517 us; the launch traced here: 516 us
  waiting for transfers between devices  371 us (72%)
  starting transfers between devices  52.2 us (10%)
  local copies, waits for them, and re-layouts  41 us (8%)
  matrix products  23.8 us (5%)
  between operations  14.2 us (3%)
  other arithmetic  13.5 us (3%)
    all_to_all x1, waiting for transfers between devices, local(): lax.all_to_all(by_head[:, :, None], 'sp', split_axis=1, concat_axis=2, ti...  180 us
    all_gather x1, waiting for transfers between devices, local(): lax.all_gather(w_latent, 'sp', axis=0, tiled=True)  81.6 us
    all_gather x1, waiting for transfers between devices, local(): lax.all_gather(paired, 'tp', axis=2, tiled=True)  52.3 us
    all_to_all x1, waiting for transfers between devices, local(): lax.all_to_all(both, 'tp', split_axis=3, concat_axis=1, tiled=True)  48.1 us
    all_to_all x1, starting transfers between devices, copy_for_each(): lax.all_to_all(jnp.broadcast_to(value[None], (peers, *value.shape)), axis...  23.7 us
    all_to_all x1, starting transfers between devices, local(): lax.all_to_all(rope_every[None, :, None], 'sp', split_axis=1, concat_axis...  12.1 us
    all_to_all x1, starting transfers between devices, local(): lax.all_to_all(by_head[:, :, None], 'sp', split_axis=1, concat_axis=2, ti...  11.6 us
    reshape x1, local copies, waits for them, and re-layouts, local(): both = both.reshape(2, prompts, rows, both.shape[2])  11.2 us
  transfers between devices with their start and end apart: 6, of which 5 were waited for; matrix products, arithmetic and copies ran while one was open for 10% of the time, Pallas kernels for 0%

commit v1 on v0

--- a/solution.py
+++ b/solution.py
@@ -6,6 +6,13 @@
 HEAD = 64
 ROPE = 32
 EPS = 1e-06
+
+
+def all_by_exchange(x, axis, dim):
+    n_dev = lax.axis_size(axis)
+    blocks = jnp.stack([x for _ in range(n_dev)])
+    blocks = lax.all_to_all(blocks, axis, split_axis=0, concat_axis=0)
+    return jnp.concatenate(blocks, axis=dim)
 
 
 def joined_along(tiles, dim):
@@ -63,10 +70,7 @@
     head_cols = w_up_key.shape[1]
     paired = jnp.stack([w_up_key, w_up_value])
     both = jnp.einsum(
-        "tk,skc->stc",
-        latent,
-        lax.all_gather(paired, "tp", axis=2, tiled=True),
-        preferred_element_type=jnp.float32,
+        "tk,skc->stc", latent, all_by_exchange(paired, "tp", 2), preferred_element_type=jnp.float32
     ).astype(jnp.bfloat16)
     both = both.reshape(2, prompts, rows, both.shape[2])
     by_head = lax.all_to_all(both, "tp", split_axis=3, concat_axis=1, tiled=True)

time: 517 us -> 471 us (0.911)
  waiting for transfers between devices: 371 us -> 320 us
  local copies, waits for them, and re-layouts: 41 us -> 52.8 us
    all_to_all x0 -> x1, waiting for transfers between devices: none -> 82.8 us  [all_by_exchange(): blocks = lax.all_to_all(blocks, axis, split_axis=0, concat_axis=0)]
    all_gather x1, waiting for transfers between devices: 81.6 us -> 0.01 us  [local(): lax.all_gather(w_latent, 'sp', axis=0, tiled=True)]
    all_gather x1 -> x0, waiting for transfers between devices: 52.3 us -> none  [local(): lax.all_gather(paired, 'tp', axis=2, tiled=True)]
    all_to_all x0 -> x1, starting transfers between devices: none -> 25.3 us  [all_by_exchange(): blocks = lax.all_to_all(blocks, axis, split_axis=0, concat_axis=0)]
    all_to_all x1, starting transfers between devices: 23.7 us -> 4.28 us  [copy_for_each(): lax.all_to_all(jnp.broadcast_to(value[None], (peers, *value.shape)), axis...]
    reshape x0 -> x1, local copies, waits for them, and re-layouts: none -> 7.78 us  [all_by_exchange(): return jnp.concatenate(blocks, axis=dim)]
    all_to_all x1, starting transfers between devices: 12.1 us -> 4.71 us  [local(): lax.all_to_all(rope_every[None, :, None], 'sp', split_axis=1, concat_axis...]
  transfers between devices with their start and end apart: 6 -> 6, of which waited for: 5 -> 4; matrix products, arithmetic and copies ran while one was open for 10% -> 12% of each run, Pallas kernels for 0% -> 0%
where the time goes in v1:
time: 471 us; the launch traced here: 470 us
  waiting for transfers between devices  320 us (68%)
  local copies, waits for them, and re-layouts  52.8 us (11%)
  starting transfers between devices  50.8 us (11%)
  matrix products  22.9 us (5%)
  between operations  14.3 us (3%)
  other arithmetic  9.49 us (2%)
    all_to_all x1, waiting for transfers between devices, local(): lax.all_to_all(by_head[:, :, None], 'sp', split_axis=1, concat_axis=2, ti...  180 us
    all_to_all x1, waiting for transfers between devices, all_by_exchange(): blocks = lax.all_to_all(blocks, axis, split_axis=0, concat_axis=0)  82.8 us
    all_to_all x1, waiting for transfers between devices, local(): lax.all_to_all(both, 'tp', split_axis=3, concat_axis=1, tiled=True)  48 us
    all_to_all x1, starting transfers between devices, all_by_exchange(): blocks = lax.all_to_all(blocks, axis, split_axis=0, concat_axis=0)  25.3 us
    all_to_all x1, starting transfers between devices, local(): lax.all_to_all(by_head[:, :, None], 'sp', split_axis=1, concat_axis=2, ti...  11.6 us
    reshape x1, local copies, waits for them, and re-layouts, local(): both = both.reshape(2, prompts, rows, both.shape[2])  11.2 us
  transfers between devices with their start and end apart: 6, of which 4 were waited for; matrix products, arithmetic and copies ran while one was open for 12% of the time, Pallas kernels for 0%

profile of v1, /device:TPU:33, one launch (start us, length us, event | category | flops | bytes accessed | tf_op | source)
XLA Modules:
  0.0 469.8 jit_solution(6129602630136782383)
XLA Ops:
  7.2 0.0 copy-start
  7.2 0.1 all-gather.2.cloned.1.call-start
  7.3 0.7 all-gather.2.cloned.1.call-update
  8.0 1.3 pad_maximum_fusion
  9.3 4.0 stack.11
  13.3 25.3 %all-to-all-start = ((bf16[8,2,1024,256]{3,2,1,0:T(8,128)(2,1)}), bf16[8,2,1024,256]{3,2,1,0:T(8,128)(2,1)}, u32[]{:S(2)}, u32[]{:S(2)}) async-start(bf16[8,2,1024,256]{3,2,1,0:T(8,128)(2,1)} %stack.11), calls=%async_computation | async-start | bytes 16777216 | tf_op jit(solution)/shard_map/all_to_all | solution.py:14
  38.7 3.3 multiply_reduce_fusion
  41.9 0.0 copy-start.3
  42.0 0.1 add_convert_fusion
  42.1 3.8 fusion.4
  45.8 0.2 fusion.21
  46.1 3.6 fusion.1
  49.7 82.8 %all-to-all-done = bf16[8,2,1024,256]{3,2,1,0:T(8,128)(2,1)} async-done(((bf16[8,2,1024,256]{3,2,1,0:T(8,128)(2,1)}), bf16[8,2,1024,256]{3,2,1,0:T(8,128)(2,1)}, u32[]{:S(2)}, u32[]{:S(2)}) %all-to-all-start) | async-done | bytes 8388640 | tf_op jit(solution)/shard_map/all_to_all | solution.py:14
  132.5 0.8 broadcast_in_dim.7
  133.3 4.3 all-to-all-start.3
  137.6 7.8 %copy.45 = bf16[8,2,128,8,256]{4,3,0,2,1:T(8,128)(2,1)} copy(bf16[8,2,128,8,256]{4,3,2,1,0:T(8,128)(2,1)} %bitcast.26) | data formatting | bytes 16777216 | tf_op jit(solution)/shard_map/reshape | solution.py:15
  145.4 8.4 %multiply_reduce_fusion.1 = (f32[512]{0:T(512)S(1)}, f32[512,1024]{1,0:T(8,128)S(1)}) fusion(bf16[512,4096]{1,0:T(8,128)(2,1)} %fusion.1, bf16[4096,1024]{1,0:T(8,128)(2,1)} %all-gather.2.cloned.1.call-done), kind=kOutput, calls=%fused_computation.14 | convolution fusion | flops 4296015360 | bytes 14682112 | tf_op jit(solution)/shard_map/dot_general | solution.py:59
  153.9 6.2 %convolution_convert_fusion = bf16[2,2048,512]{1,2,0:T(8,128)(2,1)} fusion(bf16[2,1024,2048]{2,1,0:T(8,128)(2,1)S(1)} %bitcast.71, f32[512,1024]{1,0:T(8,128)S(1)} %get-tuple-element.11, f32[1024]{0:T(1024)S(1)} %copy-done.9, f32[512]{0:T(512)S(1)} %add_rsqrt_fusion), kind=kOutput, calls=%fused_computation.12 | convolution fusion | flops 4298637312 | bytes 14686208 | tf_op jit(solution)/shard_map/tk,skc->stc/dot_general | solution.py:72
  160.1 11.2 %copy.27 = bf16[2,2,256,2048]{2,1,0,3:T(2,128)(2,1)} copy(bf16[2,2,256,2048]{3,2,1,0:T(8,128)(2,1)} %bitcast.72) | data formatting | bytes 8388608 | tf_op jit(solution)/shard_map/reshape | solution.py:75
  171.2 0.0 all-to-all-done.3
  171.2 4.9 %all-to-all-start.1 = ((bf16[2,2,256,2048]{2,1,0,3:T(2,128)(2,1)}), bf16[2,2,256,2048]{2,1,0,3:T(2,128)(2,1)}, u32[]{:S(2)}, u32[]{:S(2)}) async-start(bf16[2,2,256,2048]{2,1,0,3:T(2,128)(2,1)} %copy.27), calls=%async_computation.1 | async-start | bytes 8388608 | tf_op jit(solution)/shard_map/all_to_all | solution.py:76
  176.1 0.7 copy.32
  176.9 48.0 %all-to-all-done.1 = bf16[2,2,256,2048]{2,1,0,3:T(2,128)(2,1)} async-done(((bf16[2,2,256,2048]{2,1,0,3:T(2,128)(2,1)}), bf16[2,2,256,2048]{2,1,0,3:T(2,128)(2,1)}, u32[]{:S(2)}, u32[]{:S(2)}) %all-to-all-start.1) | async-done | bytes 4194336 | tf_op jit(solution)/shard_map/all_to_all | solution.py:76
  224.9 4.7 %all-to-all-start.4 = ((bf16[1,16,1,256,32]{3,4,2,0,1:T(8,128)(2,1)}), bf16[1,16,1,256,32]{3,4,2,0,1:T(8,128)(2,1)S(1)}, u32[]{:S(2)}, u32[]{:S(2)}) async-start(bf16[1,16,1,256,32]{3,4,2,0,1:T(8,128)(2,1)} %bitcast.14), calls=%async_computation.4 | async-start | bytes 524288 | tf_op jit(solution)/shard_map/all_to_all | solution.py:80
  229.6 4.9 %copy.28 = bf16[2,8,2,256,256]{3,4,0,2,1:T(8,128)(2,1)} copy(bf16[2,8,2,256,256]{3,2,0,4,1:T(2,128)(2,1)} %bitcast.8) | data formatting | bytes 8388608 | tf_op jit(solution)/shard_map/all_to_all | solution.py:76
  234.6 7.8 %all-to-all-done.4 = bf16[1,16,1,256,32]{3,4,2,0,1:T(8,128)(2,1)S(1)} async-done(((bf16[1,16,1,256,32]{3,4,2,0,1:T(8,128)(2,1)}), bf16[1,16,1,256,32]{3,4,2,0,1:T(8,128)(2,1)S(1)}, u32[]{:S(2)}, u32[]{:S(2)}) %all-to-all-start.4) | async-done | bytes 262176 | tf_op jit(solution)/shard_map/all_to_all | solution.py:80
  242.3 11.6 %all-to-all-start.2 = ((bf16[2,16,1,256,256]{3,4,2,0,1:T(8,128)(2,1)}), bf16[2,16,1,256,256]{3,4,2,0,1:T(8,128)(2,1)}, u32[]{:S(2)}, u32[]{:S(2)}) async-start(bf16[2,16,1,256,256]{3,4,2,0,1:T(8,128)(2,1)} %bitcast.70), calls=%async_computation.2 | async-start | bytes 8388608 | tf_op jit(solution)/shard_map/all_to_all | solution.py:79
  253.9 0.1 reshape.152
  254.0 0.5 broadcast.100
  254.5 0.7 reduce.5
  255.2 0.1 reshape.142
  255.3 0.0 copy-start.6
  255.3 180.2 %all-to-all-done.2 = bf16[2,16,1,256,256]{3,4,2,0,1:T(8,128)(2,1)} async-done(((bf16[2,16,1,256,256]{3,4,2,0,1:T(8,128)(2,1)}), bf16[2,16,1,256,256]{3,4,2,0,1:T(8,128)(2,1)}, u32[]{:S(2)}, u32[]{:S(2)}) %all-to-all-start.2) | async-done | bytes 4194336 | tf_op jit(solution)/shard_map/all_to_all | solution.py:79
  435.6 2.6 fusion.26
  438.1 0.0 copy-start.2
  438.2 1.3 copy-done.2
  439.5 2.5 copy.35
  442.0 3.9 copy.41
  445.9 2.5 copy.36
  448.4 2.4 copy.42
  450.8 4.3 reshape_reshape_squeeze.6
  455.1 2.0 fusion.28
  457.1 0.3 fusion.27
  457.3 0.2 fusion.15
  457.6 0.1 fusion.24
  457.7 2.4 reshape_reshape_squeeze.7
  460.1 2.2 fusion.13
  462.3 0.7 reshape.143
  (30 shorter events, 0.2 us)
Async XLA Ops:
  7.2 34.9 %copy-start = (bf16[4096,32]{0,1:T(8,128)(2,1)S(1)}, bf16[4096,32]{0,1:T(8,128)(2,1)}, u32[]{:S(2)}) copy-start(bf16[4096,32]{0,1:T(8,128)(2,1)} %param.14) | copy-start | bytes 786436
  7.2 138.2 %all-gather.2.cloned.1.call-start = ((), (), s32[]{:S(2)}) async-start(), calls=%async_computation.5 | async-start | bytes 8912896 | tf_op jit(solution)/shard_map/all_gather | solution.py:61
  13.3 119.1 %all-to-all-start = ((bf16[8,2,1024,256]{3,2,1,0:T(8,128)(2,1)}), bf16[8,2,1024,256]{3,2,1,0:T(8,128)(2,1)}, u32[]{:S(2)}, u32[]{:S(2)}) async-start(bf16[8,2,1024,256]{3,2,1,0:T(8,128)(2,1)} %stack.11), calls=%async_computation | async-start | bytes 16777216 | tf_op jit(solution)/shard_map/all_to_all | solution.py:14
  38.6 3.3 copy-start.10
  38.6 3.4 copy-start.7
  41.9 4.2 copy-start.3
  133.3 37.9 %all-to-all-start.3 = ((bf16[8,2,256,32]{2,1,3,0:T(2,128)(2,1)}), bf16[8,2,256,32]{2,1,3,0:T(2,128)(2,1)S(1)}, u32[]{:S(2)}, u32[]{:S(2)}) async-start(bf16[8,2,256,32]{2,1,3,0:T(2,128)(2,1)} %broadcast_in_dim.7), calls=%async_computation.3 | async-start | bytes 524288 | tf_op jit(solution)/shard_map/all_to_all | solution.py:26
  145.4 8.5 %copy-start.9 = (f32[1024]{0:T(1024)S(1)}, f32[1024]{0:T(1024)}, u32[]{:S(2)}) copy-start(f32[1024]{0:T(1024)} %param.15) | copy-start | bytes 12292
  145.4 8.5 %copy-start.4 = (bf16[8,2,128,8,256]{4,3,0,2,1:T(8,128)(2,1)S(1)}, bf16[8,2,128,8,256]{4,3,0,2,1:T(8,128)(2,1)}, u32[]{:S(2)}) copy-start(bf16[8,2,128,8,256]{4,3,0,2,1:T(8,128)(2,1)} %copy.45) | copy-start | bytes 25165828
  171.2 53.7 %all-to-all-start.1 = ((bf16[2,2,256,2048]{2,1,0,3:T(2,128)(2,1)}), bf16[2,2,256,2048]{2,1,0,3:T(2,128)(2,1)}, u32[]{:S(2)}, u32[]{:S(2)}) async-start(bf16[2,2,256,2048]{2,1,0,3:T(2,128)(2,1)} %copy.27), calls=%async_computation.1 | async-start | bytes 8388608 | tf_op jit(solution)/shard_map/all_to_all | solution.py:76
  224.9 17.4 %all-to-all-start.4 = ((bf16[1,16,1,256,32]{3,4,2,0,1:T(8,128)(2,1)}), bf16[1,16,1,256,32]{3,4,2,0,1:T(8,128)(2,1)S(1)}, u32[]{:S(2)}, u32[]{:S(2)}) async-start(bf16[1,16,1,256,32]{3,4,2,0,1:T(8,128)(2,1)} %bitcast.14), calls=%async_computation.4 | async-start | bytes 524288 | tf_op jit(solution)/shard_map/all_to_all | solution.py:80
  242.3 11.6 %copy-start.8 = (bf16[1,256]{1,0:T(2,128)(2,1)S(1)}, bf16[1,256]{1,0:T(2,128)(2,1)}, u32[]{:S(2)}) copy-start(bf16[1,256]{1,0:T(2,128)(2,1)} %param.18) | copy-start | bytes 1540
  242.3 12.2 %copy-start.11 = (bf16[1,128]{1,0:T(2,128)(2,1)S(1)}, bf16[1,128]{1,0:T(2,128)(2,1)}, u32[]{:S(2)}) copy-start(bf16[1,128]{1,0:T(2,128)(2,1)} %param.19) | copy-start | bytes 772
  242.3 193.2 %all-to-all-start.2 = ((bf16[2,16,1,256,256]{3,4,2,0,1:T(8,128)(2,1)}), bf16[2,16,1,256,256]{3,4,2,0,1:T(8,128)(2,1)}, u32[]{:S(2)}, u32[]{:S(2)}) async-start(bf16[2,16,1,256,256]{3,4,2,0,1:T(8,128)(2,1)} %bitcast.70), calls=%async_computation.2 | async-start | bytes 8388608 | tf_op jit(solution)/shard_map/all_to_all | solution.py:79
  255.3 201.8 %copy-start.6 = (bf16[4,8,16,256]{3,1,2,0:T(8,128)(2,1)}, bf16[4,8,16,256]{3,1,2,0:T(8,128)(2,1)S(1)}, u32[]{:S(2)}) copy-start(bf16[4,8,16,256]{3,1,2,0:T(8,128)(2,1)S(1)} %copy.47) | copy-start | bytes 786436
  438.1 1.3 copy-start.2
  450.7 6.9 %copy-start.5 = (bf16[1,16,1,256,256]{3,1,4,2,0:T(8,128)(2,1)S(1)}, bf16[1,16,1,256,256]{3,1,4,2,0:T(8,128)(2,1)}, u32[]{:S(2)}) copy-start(bf16[1,16,1,256,256]{3,1,4,2,0:T(8,128)(2,1)} %copy.36) | copy-start | bytes 6291460
  450.7 12.2 %copy-start.1 = (bf16[4096,32]{0,1:T(8,128)(2,1)S(1)}, bf16[4096,32]{0,1:T(8,128)(2,1)}, u32[]{:S(2)}) copy-start(bf16[4096,32]{0,1:T(8,128)(2,1)} %param.14) | copy-start | bytes 786436
Sparse Core Ops, SparseCore 0:
  9.8 118.4 all-gather.1
